TPU v7x, 32 devices: a whole 2x2x4 slice. The times are simulated.
32 devices in a mesh: grp: 2 (over x), ep: 16 (over z, y, core).
Axes of the slice: x: 2, y: 2, z: 4, core: 2. Of those that a mesh axis runs over, the one named last changes fastest.
Arguments:
- residual: bfloat16 [16, 4096], P('grp', 'ep'), parts along dimension 0, may hold values from -6 to 6
- head_states: float32 [64, 512, 1024], P(('grp', 'ep')), parts along dimension 0, may hold values from -6 to 6
- first_gain: bfloat16 [4096], replicated, may hold values from 0.099609375 to 1.8984375
- w_query: bfloat16 [4096, 2048], P(None, 'ep'), may hold values from -0.09375 to 0.09375
- w_key: bfloat16 [4096, 2048], P(None, 'ep'), may hold values from -0.09375 to 0.09375
- w_value: bfloat16 [4096, 4096], P(None, 'ep'), may hold values from -0.09375 to 0.09375
- w_gate: bfloat16 [4096, 4096], P(None, 'ep'), may hold values from -0.09375 to 0.09375
- w_low: bfloat16 [4096, 16], replicated, may hold values from -0.09375 to 0.09375
- w_decay: bfloat16 [16, 2048], replicated, may hold values from -15 to 15
- decay_bias: float32 [2048], replicated, may hold values from -40 to 4
- head_gain: bfloat16 [1024], replicated, may hold values from 0.099609375 to 1.8984375
- w_output: bfloat16 [4096, 4096], P(None, 'ep'), may hold values from -0.09375 to 0.09375
- second_gain: bfloat16 [4096], replicated, may hold values from 0.099609375 to 1.8984375
- routes: int32 [16, 2], P('grp'), parts along dimension 0, may hold values from 0 to 15, as said below
- group_logits: float32 [16, 4], P('grp'), parts along dimension 0, may hold values from -12 to 12
- expert_logits: float32 [16, 2], P('grp'), parts along dimension 0, may hold values from -9 to 9
- expert_gate: bfloat16 [16, 4096, 512], P('ep'), may hold values from -0.09375 to 0.09375
- expert_up: bfloat16 [16, 4096, 512], P('ep'), may hold values from -0.09375 to 0.09375
- expert_down: bfloat16 [16, 512, 4096], P('ep'), may hold values from -0.25 to 0.25
Outputs:
- layer_out: bfloat16 [16, 4096], P('grp', 'ep'), parts along dimension 0
- new_states: float32 [64, 512, 1024], P(('grp', 'ep')), parts along dimension 0
There are 2 independent parts, one for each index of `grp`. A program takes and returns all parts, laid end to end along the dimension named above; an argument that names none is the same for every part. Nothing has to cross between parts.
Inputs may be any that keep to these rules, and one draw needn't show every extreme that they name: `routes`: each row names 2 different experts of one group (numbers g * 4 to g * 4 + 3). No expert is named by more than 2 rows, and in every draw all experts of one group are named by exactly 2 rows.
All inputs are finite; a program needn't handle non-finite values.
Results may differ from a plain program's by a relative error of at most 0.014.
Values may be sent and summed in bfloat16 or wider, within the bound.
No kernel may reach another device: no remote copies, remote signals or barrier semaphores. Data moves between devices by JAX's collectives and lax.ppermute only.
A program may use at most 128 MiB of HBM per device.

v0:
```python
import jax
import jax.numpy as jnp
import numpy as np
from jax import lax
from jax.sharding import PartitionSpec as P

HEADS = 4
DK = 512
DV = 1024
GROUPS = 4
TOP = 2
norm_eps = 1e-06
decay_tau = 16.0


def rms_scale(values, gain):
    floats = values.astype(jnp.float32)
    return (
        floats
        * lax.rsqrt(jnp.mean(floats * floats, axis=-1, keepdims=True) + norm_eps)
        * gain.astype(jnp.float32)
    )


def route_weights(routes, group_logits, expert_logits, per_group):
    group_exp = jnp.exp(group_logits)
    group_prob = group_exp / jnp.sum(group_exp, axis=1, keepdims=True)
    chosen = routes[:, 0] // per_group
    groups_row = jnp.arange(group_logits.shape[1], dtype=jnp.int32)
    picked = jnp.sum(
        group_prob * (chosen[:, None] == groups_row[None, :]).astype(jnp.float32), axis=1
    )
    expert_exp = jnp.exp(expert_logits)
    return expert_exp / jnp.sum(expert_exp, axis=1, keepdims=True) * picked[:, None]


def per_device(
    residual,
    head_states,
    first_gain,
    w_query,
    w_key,
    w_value,
    w_gate,
    w_low,
    w_decay,
    decay_bias,
    head_gain,
    w_output,
    second_gain,
    routes,
    group_logits,
    expert_logits,
    expert_gate,
    expert_up,
    expert_down,
):
    devices = lax.axis_size("ep")
    my_index = lax.axis_index("ep")
    seq_count = residual.shape[0]
    own_width = residual.shape[1]
    width = own_width * devices
    pairs_dev = head_states.shape[0]
    slot_count = max(1, pairs_dev // HEADS)
    rows = lax.all_gather(residual, "ep", axis=1, tiled=True)
    normed = rms_scale(rows, first_gain).astype(jnp.bfloat16)
    my_head = my_index * HEADS // devices
    target = jnp.arange(devices, dtype=jnp.int32)[:, None]
    turn = jnp.arange(slot_count, dtype=jnp.int32)[None, :]
    within = jnp.mod(my_head - target * pairs_dev, HEADS) + turn * HEADS
    target_seq = (target * pairs_dev + within) // HEADS
    seq_row = jnp.arange(seq_count, dtype=jnp.int32)[None, None, :]
    picker = (target_seq[:, :, None] == seq_row) & (within < pairs_dev)[:, :, None]
    picker = picker.astype(jnp.bfloat16).reshape(devices * slot_count, seq_count)

    def outgoing(weight):
        projected = jnp.dot(normed, weight, preferred_element_type=jnp.float32).astype(jnp.bfloat16)
        placed = jnp.dot(picker, projected, preferred_element_type=jnp.float32).astype(jnp.bfloat16)
        return placed.reshape(devices, slot_count, projected.shape[1])

    send_query = outgoing(w_query)
    send_key = outgoing(w_key)
    send_value = outgoing(w_value)
    send_gate = outgoing(w_gate)
    incoming = (
        lax.all_to_all(send_query, "ep", split_axis=0, concat_axis=0, tiled=True),
        lax.all_to_all(send_key, "ep", split_axis=0, concat_axis=0, tiled=True),
        lax.all_to_all(send_value, "ep", split_axis=0, concat_axis=0, tiled=True),
        lax.all_to_all(send_gate, "ep", split_axis=0, concat_axis=0, tiled=True),
    )
    pair_ids = my_index * pairs_dev + jnp.arange(pairs_dev, dtype=jnp.int32)
    head_pick = (
        jnp.mod(pair_ids, HEADS)[:, None] == jnp.arange(HEADS, dtype=jnp.int32)[None, :]
    ).astype(jnp.bfloat16)
    turns = np.arange(pairs_dev) // HEADS
    pair_rows = np.arange(pairs_dev)

    def arrange(received):
        merged = jnp.dot(head_pick, received.reshape(HEADS, -1), preferred_element_type=jnp.float32)
        merged = merged.reshape(pairs_dev, devices // HEADS, slot_count, received.shape[2])
        return merged[pair_rows, :, turns, :].reshape(pairs_dev, -1).astype(jnp.bfloat16)

    query = arrange(incoming[0])
    key = arrange(incoming[1])
    value = arrange(incoming[2])
    gate = arrange(incoming[3])
    low = jnp.dot(normed, w_low, preferred_element_type=jnp.float32)
    decay_pre = (
        jnp.dot(low, w_decay.astype(jnp.float32), precision=lax.Precision.HIGHEST) + decay_bias
    )
    decay_pre = lax.dynamic_slice_in_dim(
        decay_pre.reshape(seq_count * HEADS, DK), my_index * pairs_dev, pairs_dev, 0
    )
    log_decay = jax.nn.log_sigmoid(decay_pre) / decay_tau
    new_states = (
        head_states * jnp.exp(log_decay)[:, :, None]
        + key.astype(jnp.float32)[:, :, None] * value.astype(jnp.float32)[:, None, :]
    )
    read = jnp.einsum(
        "pk,pkv->pv",
        query.astype(jnp.float32) * DK ** (-0.5),
        new_states,
        precision=lax.Precision.HIGHEST,
    )
    mixed = (rms_scale(read, head_gain) * jax.nn.silu(gate.astype(jnp.float32))).astype(
        jnp.bfloat16
    )
    gathered = lax.all_gather(mixed, "ep", axis=0, tiled=True).reshape(seq_count, HEADS * DV)
    branch = jnp.dot(gathered, w_output, preferred_element_type=jnp.float32).astype(jnp.bfloat16)
    stream = (residual.astype(jnp.float32) + branch.astype(jnp.float32)).astype(jnp.bfloat16)
    floats = stream.astype(jnp.float32)
    total = lax.psum(jnp.sum(floats * floats, axis=1), "ep")
    gain_part = lax.dynamic_slice_in_dim(second_gain, my_index * own_width, own_width)
    scaled = floats * lax.rsqrt(total / width + norm_eps)[:, None] * gain_part.astype(jnp.float32)
    expert_in = lax.all_gather(scaled.astype(jnp.bfloat16), "ep", axis=1, tiled=True)
    capacity = 2 * seq_count * TOP // devices
    weights = route_weights(routes, group_logits, expert_logits, devices // GROUPS)
    hits = (routes == my_index).astype(jnp.int32)
    mine = jnp.sum(weights * hits.astype(jnp.float32), axis=1)
    routed = jnp.sum(hits, axis=1)
    slot = jnp.cumsum(routed) - routed
    chooser = (slot[None, :] == jnp.arange(capacity, dtype=jnp.int32)[:, None]) & (
        routed[None, :] > 0
    )
    picked = jnp.dot(
        chooser.astype(jnp.bfloat16), expert_in, preferred_element_type=jnp.float32
    ).astype(jnp.bfloat16)
    row_weight = jnp.dot(chooser.astype(jnp.float32), mine, precision=lax.Precision.HIGHEST)
    gate_part = jnp.dot(picked, expert_gate[0], preferred_element_type=jnp.float32)
    up_part = jnp.dot(picked, expert_up[0], preferred_element_type=jnp.float32)
    active = (jax.nn.silu(gate_part) * up_part * row_weight[:, None]).astype(jnp.bfloat16)
    expert_rows = jnp.dot(active, expert_down[0], preferred_element_type=jnp.float32).astype(
        jnp.bfloat16
    )
    arrived = lax.all_to_all(expert_rows, "ep", split_axis=1, concat_axis=0, tiled=True)
    every = jnp.arange(devices, dtype=jnp.int32)
    hit_all = jnp.sum((routes[:, :, None] == every[None, None, :]).astype(jnp.int32), axis=1)
    slot_all = jnp.cumsum(hit_all, axis=0) - hit_all
    placer = (slot_all[:, :, None] == jnp.arange(capacity, dtype=jnp.int32)[None, None, :]) & (
        hit_all[:, :, None] > 0
    )
    placer = placer.astype(jnp.bfloat16).reshape(seq_count, devices * capacity)
    returned = jnp.dot(placer, arrived, preferred_element_type=jnp.float32)
    layer_out = (stream.astype(jnp.float32) + returned).astype(jnp.bfloat16)
    return (layer_out, new_states)


def solution(mesh):
    return jax.shard_map(
        per_device,
        mesh=mesh,
        in_specs=(
            P("grp", "ep"),
            P(("grp", "ep"), None, None),
            P(),
            P(None, "ep"),
            P(None, "ep"),
            P(None, "ep"),
            P(None, "ep"),
            P(),
            P(),
            P(),
            P(),
            P(None, "ep"),
            P(),
            P("grp", None),
            P("grp", None),
            P("grp", None),
            P("ep", None, None),
            P("ep", None, None),
            P("ep", None, None),
        ),
        out_specs=(P("grp", "ep"), P(("grp", "ep"), None, None)),
        check_vma=False,
    )
```

profile of v0, /device:TPU:0, one launch (start us, length us, event | category | flops | bytes accessed | tf_op | source)
XLA Modules:
  0.0 169.2 jit_solution(12246803465482614124)
XLA Ops:
  0.7 23.7 %all_gather.9 = bf16[8,4096]{1,0:T(8,128)(2,1)S(1)} all-gather(bf16[8,256]{1,0:T(8,128)(2,1)} %param.29), channel_id=1, replica_groups=mesh['grp'=2,'ep'=16] {'ep'}, dimensions={1}, use_global_device_ids=true | all-gather | bytes 69632 | tf_op jit(solution)/shard_map/all_gather | solution.py:65
  24.4 0.1 fusion.26
  24.6 0.7 convert_element_type.145
  25.3 1.6 fusion.14
  26.9 0.6 copy.61
  27.5 3.4 %all-to-all-start.1 = ((bf16[16,1,128]{2,1,0:T(2,128)(2,1)}), bf16[16,1,128]{2,1,0:T(2,128)(2,1)S(1)}, u32[]{:S(2)}, u32[]{:S(2)}) async-start(bf16[16,1,128]{2,1,0:T(2,128)(2,1)} %copy.61), calls=%async_computation.1 | async-start | bytes 16384 | tf_op jit(solution)/shard_map/all_to_all | solution.py:87
  31.0 0.7 fusion.70
  31.7 0.7 fusion.73
  32.4 0.8 convert_reduce_fusion
  33.1 0.5 fusion.5
  33.6 1.1 fusion.88
  34.8 1.0 convolution_add_fusion
  35.8 1.6 fusion.13
  37.4 2.1 %fusion.6 = bf16[16,1,256]{2,0,1:T(8,128)(2,1)S(1)} fusion(bf16[4096,256]{1,0:T(8,128)(2,1)} %param.35, s32[16]{0:T(128)S(1)} %and_select_fusion.1, pred[16]{0:T(512)(128)(4,1)S(1)} %broadcast_compare_fusion.2, bf16[8,4096]{1,0:T(8,128)(2,1)S(1)} %all_gather.9, f32[4096]{0:T(1024)S(1)} %convert_element_type.145, f32[8]{0:T(128)S(1)} %add_rsqrt_fusion.2), kind=kOutput, calls=%fused_computation.16 | convolution fusion | flops 16980224 | bytes 2187376 | tf_op jit(solution)/shard_map/dot_general | solution.py:78
  39.6 0.2 reduce-window.8
  39.9 0.8 dynamic-slice_convert_fusion
  40.8 0.5 broadcast.372
  41.3 0.6 reduce.5
  42.0 0.6 reshape.330
  42.6 0.6 copy.59
  43.2 0.6 reduce.4
  43.9 0.6 reshape.328
  44.5 6.0 %all-to-all-start = ((bf16[16,1,128]{2,1,0:T(2,128)(2,1)}), bf16[16,1,128]{2,1,0:T(2,128)(2,1)S(1)}, u32[]{:S(2)}, u32[]{:S(2)}) async-start(bf16[16,1,128]{2,1,0:T(2,128)(2,1)} %copy.59), calls=%async_computation | async-start | bytes 16384 | tf_op jit(solution)/shard_map/all_to_all | solution.py:86
  50.5 0.2 convolution_bitcast_fusion.3
  50.7 0.6 gather_fusion.1
  51.3 5.5 %all-to-all-done = bf16[16,1,128]{2,1,0:T(2,128)(2,1)S(1)} async-done(((bf16[16,1,128]{2,1,0:T(2,128)(2,1)}), bf16[16,1,128]{2,1,0:T(2,128)(2,1)S(1)}, u32[]{:S(2)}, u32[]{:S(2)}) %all-to-all-start) | async-done | bytes 4128 | tf_op jit(solution)/shard_map/all_to_all | solution.py:86
  56.8 3.4 %all-to-all-start.2 = ((bf16[16,2,128]{2,1,0:T(2,128)(2,1)}), bf16[16,2,128]{2,1,0:T(2,128)(2,1)S(1)}, u32[]{:S(2)}, u32[]{:S(2)}) async-start(bf16[16,2,128]{2,1,0:T(2,128)(2,1)} %reshape.330), calls=%async_computation.2 | async-start | bytes 16384 | tf_op jit(solution)/shard_map/all_to_all | solution.py:88
  60.3 0.2 convolution_bitcast_fusion.4
  60.5 0.6 gather_fusion
  61.1 5.6 %all-to-all-done.2 = bf16[16,2,128]{2,1,0:T(2,128)(2,1)S(1)} async-done(((bf16[16,2,128]{2,1,0:T(2,128)(2,1)}), bf16[16,2,128]{2,1,0:T(2,128)(2,1)S(1)}, u32[]{:S(2)}, u32[]{:S(2)}) %all-to-all-start.2) | async-done | bytes 8224 | tf_op jit(solution)/shard_map/all_to_all | solution.py:88
  66.6 3.5 %all-to-all-start.3 = ((bf16[16,2,128]{2,1,0:T(2,128)(2,1)}), bf16[16,2,128]{2,1,0:T(2,128)(2,1)S(1)}, u32[]{:S(2)}, u32[]{:S(2)}) async-start(bf16[16,2,128]{2,1,0:T(2,128)(2,1)} %reshape.328), calls=%async_computation.3 | async-start | bytes 16384 | tf_op jit(solution)/shard_map/all_to_all | solution.py:89
  70.2 0.2 convolution_bitcast_fusion.2
  70.4 0.6 gather_fusion.2
  71.0 2.7 %multiply_add_fusion = f32[2,512,1024]{2,1,0:T(8,128)S(1)} fusion(f32[2,512,1024]{2,1,0:T(8,128)} %param.30, f32[2,1024]{1,0:T(2,128)S(1)} %bitcast.122, f32[2,512]{1,0:T(2,128)S(1)} %bitcast.124, f32[2,512]{1,0:T(2,128)S(1)} %fusion.44), kind=kLoop, calls=%fused_computation.11 | loop fusion | flops 3145728 | bytes 8404992 | tf_op jit(solution)/shard_map/add | solution.py:116
  73.8 2.0 %copy-done.1 = f32[2,512,1024]{2,1,0:T(8,128)} copy-done((f32[2,512,1024]{2,1,0:T(8,128)}, f32[2,512,1024]{2,1,0:T(8,128)S(1)}, u32[]{:S(2)}) %copy-start.1) | copy-done | bytes 4194328
  75.8 2.1 %fusion.92 = f32[2,1,1024]{2,1,0:T(1,128)S(1)} fusion(f32[2,512,1]{1,2,0:T(1,128)S(1)} %bitcast.123, f32[2,512,1024]{2,1,0:T(8,128)S(1)} %multiply_add_fusion), kind=kOutput, calls=%fused_computation.142 | convolution fusion | flops 12582912 | bytes 4206592 | tf_op jit(solution)/shard_map/pk,pkv->pv/dot_general | solution.py:119
  78.1 0.2 convolution_bitcast_fusion.1
  78.3 0.6 gather_fusion.3
  78.9 21.8 %all-gather = bf16[16,2,1024]{2,1,0:T(2,128)(2,1)S(1)} all-gather(bf16[1,2,1024]{2,1,0:T(2,128)(2,1)S(1)} %fusion.60), channel_id=1, replica_groups=mesh['grp'=2,'ep'=16] {'ep'}, dimensions={0}, use_global_device_ids=true | all-gather | bytes 69632 | tf_op jit(solution)/shard_map/all_gather | solution.py:128
  100.8 2.1 %multiply_reduce_fusion = (f32[8]{0:T(128)S(1)}, f32[8,256]{1,0:T(8,128)S(1)}) fusion(bf16[8,4096]{1,0:T(8,128)(2,1)S(1)} %reshape.284, bf16[4096,256]{1,0:T(8,128)(2,1)} %param.40, bf16[8,256]{1,0:T(8,128)(2,1)S(1)} %copy-done.2), kind=kOutput, calls=%fused_computation.58 | convolution fusion | flops 16793592 | bytes 2175008 | tf_op jit(solution)/shard_map/dot_general | solution.py:129
  102.9 29.8 %psum.7 = f32[8]{0:T(128)S(1)} all-reduce(f32[8]{0:T(128)S(1)} %get-tuple-element.2), channel_id=1, replica_groups=mesh['grp'=2,'ep'=16] {'ep'}, use_global_device_ids=true, to_apply=%region_7.8 | all-reduce | flops 8 | bytes 64 | tf_op jit(solution)/shard_map/psum | solution.py:132
  132.8 17.3 %all_gather.11 = bf16[8,4096]{1,0:T(8,128)(2,1)S(1)} all-gather(bf16[8,256]{1,0:T(8,128)(2,1)S(1)} %multiply_convert_fusion), channel_id=1, replica_groups=mesh['grp'=2,'ep'=16] {'ep'}, dimensions={1}, use_global_device_ids=true | all-gather | bytes 69632 | tf_op jit(solution)/shard_map/all_gather | solution.py:135
  150.1 0.1 convolution_convert_fusion.1
  150.2 2.8 %fusion.3 = f32[2,512]{1,0:T(2,128)S(1)} fusion(bf16[2,4096]{1,0:T(2,128)(2,1)S(1)} %convolution_convert_fusion.1, bf16[1,4096,512]{2,1,0:T(8,128)(2,1)} %param.45), kind=kOutput, calls=%fused_computation.9 | convolution fusion | flops 8388608 | bytes 4214784 | tf_op jit(solution)/shard_map/dot_general | solution.py:149
  153.1 5.4 %convolution_convert_fusion = bf16[2,4096]{1,0:T(2,128)(2,1)} fusion(bf16[1,512,4096]{2,1,0:T(8,128)(2,1)} %param.47, bf16[2,4096]{1,0:T(2,128)(2,1)S(1)} %convolution_convert_fusion.1, bf16[1,4096,512]{2,1,0:T(8,128)(2,1)} %param.46, f32[2,512]{1,0:T(2,128)S(1)} %fusion.3, f32[2]{0:T(128)S(1)} %convolution_bitcast_fusion.5), kind=kOutput, calls=%fused_computation.4 | convolution fusion | flops 16792576 | bytes 8425480 | tf_op jit(solution)/shard_map/dot_general | solution.py:152
  158.4 3.5 %all-to-all-start.4 = ((bf16[2,16,256]{2,0,1:T(2,128)(2,1)}), bf16[2,16,256]{2,0,1:T(2,128)(2,1)S(1)}, u32[]{:S(2)}, u32[]{:S(2)}) async-start(bf16[2,16,256]{2,0,1:T(2,128)(2,1)} %bitcast.28), calls=%async_computation.4 | async-start | bytes 32768 | tf_op jit(solution)/shard_map/all_to_all | solution.py:155
  162.0 6.4 %all-to-all-done.4 = bf16[2,16,256]{2,0,1:T(2,128)(2,1)S(1)} async-done(((bf16[2,16,256]{2,0,1:T(2,128)(2,1)}), bf16[2,16,256]{2,0,1:T(2,128)(2,1)S(1)}, u32[]{:S(2)}, u32[]{:S(2)}) %all-to-all-start.4) | async-done | bytes 16416 | tf_op jit(solution)/shard_map/all_to_all | solution.py:155
  168.4 0.8 fusion.8
  (60 shorter events, 1.1 us)
Async XLA Ops:
  0.6 32.5 %copy-start = (bf16[4096,256]{1,0:T(8,128)(2,1)S(1)}, bf16[4096,256]{1,0:T(8,128)(2,1)}, u32[]{:S(2)}) copy-start(bf16[4096,256]{1,0:T(8,128)(2,1)} %param.34) | copy-start | bytes 6291460
  0.6 40.0 %copy-start.3 = (s32[8,2]{0,1:T(2,128)S(1)}, s32[8,2]{0,1:T(2,128)}, u32[]{:S(2)}) copy-start(s32[8,2]{0,1:T(2,128)} %param.42) | copy-start | bytes 196
  0.7 39.1 %copy-start.4 = (f32[8,4]{0,1:T(4,128)S(1)}, f32[8,4]{0,1:T(4,128)}, u32[]{:S(2)}) copy-start(f32[8,4]{0,1:T(4,128)} %param.43) | copy-start | bytes 388
  0.7 39.1 %copy-start.6 = (f32[8,2]{0,1:T(2,128)S(1)}, f32[8,2]{0,1:T(2,128)}, u32[]{:S(2)}) copy-start(f32[8,2]{0,1:T(2,128)} %param.44) | copy-start | bytes 196
  0.7 43.8 %copy-start.5 = (bf16[1024]{0:T(1024)(128)(2,1)S(1)}, bf16[1024]{0:T(1024)(128)(2,1)}, u32[]{:S(2)}) copy-start(bf16[1024]{0:T(1024)(128)(2,1)} %param.39) | copy-start | bytes 6148
  27.5 16.9 %all-to-all-start.1 = ((bf16[16,1,128]{2,1,0:T(2,128)(2,1)}), bf16[16,1,128]{2,1,0:T(2,128)(2,1)S(1)}, u32[]{:S(2)}, u32[]{:S(2)}) async-start(bf16[16,1,128]{2,1,0:T(2,128)(2,1)} %copy.61), calls=%async_computation.1 | async-start | bytes 16384 | tf_op jit(solution)/shard_map/all_to_all | solution.py:87
  44.5 12.3 %all-to-all-start = ((bf16[16,1,128]{2,1,0:T(2,128)(2,1)}), bf16[16,1,128]{2,1,0:T(2,128)(2,1)S(1)}, u32[]{:S(2)}, u32[]{:S(2)}) async-start(bf16[16,1,128]{2,1,0:T(2,128)(2,1)} %copy.59), calls=%async_computation | async-start | bytes 16384 | tf_op jit(solution)/shard_map/all_to_all | solution.py:86
  56.8 9.8 %all-to-all-start.2 = ((bf16[16,2,128]{2,1,0:T(2,128)(2,1)}), bf16[16,2,128]{2,1,0:T(2,128)(2,1)S(1)}, u32[]{:S(2)}, u32[]{:S(2)}) async-start(bf16[16,2,128]{2,1,0:T(2,128)(2,1)} %reshape.330), calls=%async_computation.2 | async-start | bytes 16384 | tf_op jit(solution)/shard_map/all_to_all | solution.py:88
  66.6 11.3 %all-to-all-start.3 = ((bf16[16,2,128]{2,1,0:T(2,128)(2,1)}), bf16[16,2,128]{2,1,0:T(2,128)(2,1)S(1)}, u32[]{:S(2)}, u32[]{:S(2)}) async-start(bf16[16,2,128]{2,1,0:T(2,128)(2,1)} %reshape.328), calls=%async_computation.3 | async-start | bytes 16384 | tf_op jit(solution)/shard_map/all_to_all | solution.py:89
  73.7 2.0 %copy-start.1 = (f32[2,512,1024]{2,1,0:T(8,128)}, f32[2,512,1024]{2,1,0:T(8,128)S(1)}, u32[]{:S(2)}) copy-start(f32[2,512,1024]{2,1,0:T(8,128)S(1)} %multiply_add_fusion) | copy-start | bytes 12582916
  73.8 27.0 %copy-start.2 = (bf16[8,256]{1,0:T(8,128)(2,1)S(1)}, bf16[8,256]{1,0:T(8,128)(2,1)}, u32[]{:S(2)}) copy-start(bf16[8,256]{1,0:T(8,128)(2,1)} %param.29) | copy-start | bytes 12292
  158.4 10.0 %all-to-all-start.4 = ((bf16[2,16,256]{2,0,1:T(2,128)(2,1)}), bf16[2,16,256]{2,0,1:T(2,128)(2,1)S(1)}, u32[]{:S(2)}, u32[]{:S(2)}) async-start(bf16[2,16,256]{2,0,1:T(2,128)(2,1)} %bitcast.28), calls=%async_computation.4 | async-start | bytes 32768 | tf_op jit(solution)/shard_map/all_to_all | solution.py:155
where the time goes:
time: 170 us; the launch traced here: 169 us
  blocking collectives  92.6 us (54%)
  matrix products  22.2 us (13%)
  starting transfers between devices  19.8 us (12%)
  waiting for transfers between devices  17.5 us (10%)
  other arithmetic  8.69 us (5%)
  local copies, waits for them, and re-layouts  7.43 us (4%)
    psum x1, blocking collectives, per_device(): total = lax.psum(jnp.sum(floats * floats, axis=1), 'ep')  29.8 us
    all_gather x1, blocking collectives, per_device(): rows = lax.all_gather(residual, 'ep', axis=1, tiled=True)  23.7 us
    all_gather x1, blocking collectives, per_device(): lax.all_gather(mixed, 'ep', axis=0, tiled=True)  21.8 us
    all_gather x1, blocking collectives, per_device(): lax.all_gather(scaled.astype(jnp.bfloat16), 'ep', axis=1, tiled=True)  17.3 us
    all_to_all x1, waiting for transfers between devices, per_device(): lax.all_to_all(expert_rows, 'ep', split_axis=1, concat_axis=0, tiled=True)  6.42 us
    all_to_all x1, starting transfers between devices, per_device(): lax.all_to_all(send_query, 'ep', split_axis=0, concat_axis=0, tiled=True)  5.98 us
    dot_general x4, matrix products, outgoing(): jnp.dot(picker, projected, preferred_element_type=jnp.float32)  5.92 us
    all_to_all x1, waiting for transfers between devices, per_device(): lax.all_to_all(send_value, 'ep', split_axis=0, concat_axis=0, tiled=True)  5.56 us
  transfers between devices with their start and end apart: 5, of which 3 were waited for; matrix products, arithmetic and copies ran while one was open for 12% of the time, Pallas kernels for 0%

commit v1 on v0

--- a/solution.py
+++ b/solution.py
@@ -152,7 +152,10 @@
     expert_rows = jnp.dot(active, expert_down[0], preferred_element_type=jnp.float32).astype(
         jnp.bfloat16
     )
-    arrived = lax.all_to_all(expert_rows, "ep", split_axis=1, concat_axis=0, tiled=True)
+    arrived = jnp.concatenate(
+        lax.all_to_all(jnp.stack(jnp.split(expert_rows, lax.axis_size("ep"), axis=1)), "ep", 0, 0),
+        axis=0,
+    )
     every = jnp.arange(devices, dtype=jnp.int32)
     hit_all = jnp.sum((routes[:, :, None] == every[None, None, :]).astype(jnp.int32), axis=1)
     slot_all = jnp.cumsum(hit_all, axis=0) - hit_all

time: 170 us -> 179 us (1.053)
  local copies, waits for them, and re-layouts: 7.43 us -> 16.7 us
    unnamed x21 -> x36, local copies, waits for them, and re-layouts: 3.27 us -> 11.9 us
where the time goes in v1:
time: 179 us; the launch traced here: 178 us
  blocking collectives  92.6 us (52%)
  matrix products  21.6 us (12%)
  starting transfers between devices  19.8 us (11%)
  waiting for transfers between devices  17.5 us (10%)
  local copies, waits for them, and re-layouts  16.7 us (9%)
  other arithmetic  8.69 us (5%)
    psum x1, blocking collectives, per_device(): total = lax.psum(jnp.sum(floats * floats, axis=1), 'ep')  29.8 us
    all_gather x1, blocking collectives, per_device(): rows = lax.all_gather(residual, 'ep', axis=1, tiled=True)  23.7 us
    all_gather x1, blocking collectives, per_device(): lax.all_gather(mixed, 'ep', axis=0, tiled=True)  21.8 us
    all_gather x1, blocking collectives, per_device(): lax.all_gather(scaled.astype(jnp.bfloat16), 'ep', axis=1, tiled=True)  17.3 us
    unnamed x36, local copies, waits for them, and re-layouts  11.9 us
    all_to_all x1, waiting for transfers between devices, per_device(): lax.all_to_all(jnp.stack(jnp.split(expert_rows, lax.axis_size('ep'), axis...  6.42 us
    all_to_all x1, starting transfers between devices, per_device(): lax.all_to_all(send_query, 'ep', split_axis=0, concat_axis=0, tiled=True)  5.98 us
    dot_general x4, matrix products, outgoing(): jnp.dot(picker, projected, preferred_element_type=jnp.float32)  5.92 us
  transfers between devices with their start and end apart: 5, of which 3 were waited for; matrix products, arithmetic and copies ran while one was open for 12% of the time, Pallas kernels for 0%

profile of v1, /device:TPU:0, one launch (start us, length us, event | category | flops | bytes accessed | tf_op | source)
XLA Modules:
  0.0 177.8 jit_solution(13739551876777802191)
XLA Ops:
  0.7 23.7 %all_gather.9 = bf16[8,4096]{1,0:T(8,128)(2,1)S(1)} all-gather(bf16[8,256]{1,0:T(8,128)(2,1)} %param.29), channel_id=1, replica_groups=mesh['grp'=2,'ep'=16] {'ep'}, dimensions={1}, use_global_device_ids=true | all-gather | bytes 69632 | tf_op jit(solution)/shard_map/all_gather | solution.py:65
  24.6 0.7 convert_element_type.145
  25.3 1.6 fusion.14
  26.9 0.6 copy.61
  27.5 3.4 %all-to-all-start.1 = ((bf16[16,1,128]{2,1,0:T(2,128)(2,1)}), bf16[16,1,128]{2,1,0:T(2,128)(2,1)S(1)}, u32[]{:S(2)}, u32[]{:S(2)}) async-start(bf16[16,1,128]{2,1,0:T(2,128)(2,1)} %copy.61), calls=%async_computation.1 | async-start | bytes 16384 | tf_op jit(solution)/shard_map/all_to_all | solution.py:87
  31.0 0.7 fusion.69
  31.7 0.7 fusion.72
  32.4 0.8 convert_reduce_fusion
  33.6 1.1 fusion.87
  34.8 1.0 convolution_add_fusion
  35.8 1.6 fusion.13
  37.4 2.1 %fusion.6 = bf16[16,1,256]{2,0,1:T(8,128)(2,1)S(1)} fusion(bf16[4096,256]{1,0:T(8,128)(2,1)} %param.35, s32[16]{0:T(128)S(1)} %and_select_fusion.1, pred[16]{0:T(512)(128)(4,1)S(1)} %broadcast_compare_fusion.2, bf16[8,4096]{1,0:T(8,128)(2,1)S(1)} %all_gather.9, f32[4096]{0:T(1024)S(1)} %convert_element_type.145, f32[8]{0:T(128)S(1)} %add_rsqrt_fusion.2), kind=kOutput, calls=%fused_computation.16 | convolution fusion | flops 16980224 | bytes 2187376 | tf_op jit(solution)/shard_map/dot_general | solution.py:78
  39.9 0.8 dynamic-slice_convert_fusion
  41.3 0.6 reduce.5
  42.0 0.6 reshape.328
  42.6 0.6 copy.59
  43.2 0.6 reduce.4
  43.9 0.6 reshape.326
  44.5 6.0 %all-to-all-start = ((bf16[16,1,128]{2,1,0:T(2,128)(2,1)}), bf16[16,1,128]{2,1,0:T(2,128)(2,1)S(1)}, u32[]{:S(2)}, u32[]{:S(2)}) async-start(bf16[16,1,128]{2,1,0:T(2,128)(2,1)} %copy.59), calls=%async_computation | async-start | bytes 16384 | tf_op jit(solution)/shard_map/all_to_all | solution.py:86
  51.3 5.5 %all-to-all-done = bf16[16,1,128]{2,1,0:T(2,128)(2,1)S(1)} async-done(((bf16[16,1,128]{2,1,0:T(2,128)(2,1)}), bf16[16,1,128]{2,1,0:T(2,128)(2,1)S(1)}, u32[]{:S(2)}, u32[]{:S(2)}) %all-to-all-start) | async-done | bytes 4128 | tf_op jit(solution)/shard_map/all_to_all | solution.py:86
  56.8 3.4 %all-to-all-start.2 = ((bf16[16,2,128]{2,1,0:T(2,128)(2,1)}), bf16[16,2,128]{2,1,0:T(2,128)(2,1)S(1)}, u32[]{:S(2)}, u32[]{:S(2)}) async-start(bf16[16,2,128]{2,1,0:T(2,128)(2,1)} %reshape.328), calls=%async_computation.2 | async-start | bytes 16384 | tf_op jit(solution)/shard_map/all_to_all | solution.py:88
  61.1 5.6 %all-to-all-done.2 = bf16[16,2,128]{2,1,0:T(2,128)(2,1)S(1)} async-done(((bf16[16,2,128]{2,1,0:T(2,128)(2,1)}), bf16[16,2,128]{2,1,0:T(2,128)(2,1)S(1)}, u32[]{:S(2)}, u32[]{:S(2)}) %all-to-all-start.2) | async-done | bytes 8224 | tf_op jit(solution)/shard_map/all_to_all | solution.py:88
  66.6 3.5 %all-to-all-start.3 = ((bf16[16,2,128]{2,1,0:T(2,128)(2,1)}), bf16[16,2,128]{2,1,0:T(2,128)(2,1)S(1)}, u32[]{:S(2)}, u32[]{:S(2)}) async-start(bf16[16,2,128]{2,1,0:T(2,128)(2,1)} %reshape.326), calls=%async_computation.3 | async-start | bytes 16384 | tf_op jit(solution)/shard_map/all_to_all | solution.py:89
  70.4 0.6 gather_fusion.2
  71.0 2.7 %multiply_add_fusion = f32[2,512,1024]{2,1,0:T(8,128)S(1)} fusion(f32[2,512,1024]{2,1,0:T(8,128)} %param.30, f32[2,1024]{1,0:T(2,128)S(1)} %bitcast.182, f32[2,512]{1,0:T(2,128)S(1)} %bitcast.184, f32[2,512]{1,0:T(2,128)S(1)} %fusion.43), kind=kLoop, calls=%fused_computation.11 | loop fusion | flops 3145728 | bytes 8404992 | tf_op jit(solution)/shard_map/add | solution.py:116
  73.8 2.0 %copy-done.1 = f32[2,512,1024]{2,1,0:T(8,128)} copy-done((f32[2,512,1024]{2,1,0:T(8,128)}, f32[2,512,1024]{2,1,0:T(8,128)S(1)}, u32[]{:S(2)}) %copy-start.1) | copy-done | bytes 4194328
  75.8 2.1 %fusion.91 = f32[2,1,1024]{2,1,0:T(1,128)S(1)} fusion(f32[2,512,1]{1,2,0:T(1,128)S(1)} %bitcast.183, f32[2,512,1024]{2,1,0:T(8,128)S(1)} %multiply_add_fusion), kind=kOutput, calls=%fused_computation.173 | convolution fusion | flops 12582912 | bytes 4206592 | tf_op jit(solution)/shard_map/pk,pkv->pv/dot_general | solution.py:119
  78.3 0.6 gather_fusion.3
  78.9 21.8 %all-gather = bf16[16,2,1024]{2,1,0:T(2,128)(2,1)S(1)} all-gather(bf16[1,2,1024]{2,1,0:T(2,128)(2,1)S(1)} %fusion.59), channel_id=1, replica_groups=mesh['grp'=2,'ep'=16] {'ep'}, dimensions={0}, use_global_device_ids=true | all-gather | bytes 69632 | tf_op jit(solution)/shard_map/all_gather | solution.py:128
  100.8 2.1 %multiply_reduce_fusion = (f32[8]{0:T(128)S(1)}, f32[8,256]{1,0:T(8,128)S(1)}) fusion(bf16[8,4096]{1,0:T(8,128)(2,1)S(1)} %reshape.282, bf16[4096,256]{1,0:T(8,128)(2,1)} %param.40, bf16[8,256]{1,0:T(8,128)(2,1)S(1)} %copy-done.2), kind=kOutput, calls=%fused_computation.73 | convolution fusion | flops 16793592 | bytes 2175008 | tf_op jit(solution)/shard_map/dot_general | solution.py:129
  102.9 29.8 %psum.7 = f32[8]{0:T(128)S(1)} all-reduce(f32[8]{0:T(128)S(1)} %get-tuple-element.2), channel_id=1, replica_groups=mesh['grp'=2,'ep'=16] {'ep'}, use_global_device_ids=true, to_apply=%region_7.8 | all-reduce | flops 8 | bytes 64 | tf_op jit(solution)/shard_map/psum | solution.py:132
  132.8 17.3 %all_gather.11 = bf16[8,4096]{1,0:T(8,128)(2,1)S(1)} all-gather(bf16[8,256]{1,0:T(8,128)(2,1)S(1)} %multiply_convert_fusion), channel_id=1, replica_groups=mesh['grp'=2,'ep'=16] {'ep'}, dimensions={1}, use_global_device_ids=true | all-gather | bytes 69632 | tf_op jit(solution)/shard_map/all_gather | solution.py:135
  150.2 2.8 %fusion.3 = f32[2,512]{1,0:T(2,128)S(1)} fusion(bf16[2,4096]{1,0:T(2,128)(2,1)S(1)} %convolution_convert_fusion.1, bf16[1,4096,512]{2,1,0:T(8,128)(2,1)} %param.45), kind=kOutput, calls=%fused_computation.9 | convolution fusion | flops 8388608 | bytes 4214784 | tf_op jit(solution)/shard_map/dot_general | solution.py:149
  153.1 4.8 %convolution_convert_fusion = bf16[2,4096]{1,0:T(2,128)(2,1)S(1)} fusion(bf16[1,512,4096]{2,1,0:T(8,128)(2,1)} %param.47, bf16[2,4096]{1,0:T(2,128)(2,1)S(1)} %convolution_convert_fusion.1, bf16[1,4096,512]{2,1,0:T(8,128)(2,1)} %param.46, f32[2,512]{1,0:T(2,128)S(1)} %fusion.3, f32[2]{0:T(128)S(1)} %convolution_bitcast_fusion.5), kind=kOutput, calls=%fused_computation.4 | convolution fusion | flops 16792576 | bytes 8425480 | tf_op jit(solution)/shard_map/dot_general | solution.py:152
  157.8 0.6 constant_dynamic-update-slice_fusion.15
  158.4 0.6 constant_dynamic-update-slice_fusion.14
  159.0 0.6 constant_dynamic-update-slice_fusion.13
  160.2 0.6 constant_dynamic-update-slice_fusion.11
  160.8 0.6 constant_dynamic-update-slice_fusion.10
  161.9 0.6 constant_dynamic-update-slice_fusion.8
  162.5 0.6 constant_dynamic-update-slice_fusion.7
  163.6 0.6 constant_dynamic-update-slice_fusion.5
  164.2 0.6 constant_dynamic-update-slice_fusion.4
  165.9 0.6 constant_dynamic-update-slice_fusion.1
  166.5 0.6 constant_dynamic-update-slice_fusion
  167.1 3.5 %all-to-all-start.4 = ((bf16[16,2,256]{2,1,0:T(2,128)(2,1)}), bf16[16,2,256]{2,1,0:T(2,128)(2,1)S(1)}, u32[]{:S(2)}, u32[]{:S(2)}) async-start(bf16[16,2,256]{2,1,0:T(2,128)(2,1)} %constant_dynamic-update-slice_fusion), calls=%async_computation.4 | async-start | bytes 32768 | tf_op jit(solution)/shard_map/all_to_all | solution.py:156
  170.6 6.4 %all-to-all-done.4 = bf16[16,2,256]{2,1,0:T(2,128)(2,1)S(1)} async-done(((bf16[16,2,256]{2,1,0:T(2,128)(2,1)}), bf16[16,2,256]{2,1,0:T(2,128)(2,1)S(1)}, u32[]{:S(2)}, u32[]{:S(2)}) %all-to-all-start.4) | async-done | bytes 16416 | tf_op jit(solution)/shard_map/all_to_all | solution.py:156
  177.0 0.8 fusion.8
  (76 shorter events, 7.3 us)
Async XLA Ops:
  0.6 32.5 %copy-start = (bf16[4096,256]{1,0:T(8,128)(2,1)S(1)}, bf16[4096,256]{1,0:T(8,128)(2,1)}, u32[]{:S(2)}) copy-start(bf16[4096,256]{1,0:T(8,128)(2,1)} %param.34) | copy-start | bytes 6291460
  0.6 40.0 %copy-start.3 = (s32[8,2]{0,1:T(2,128)S(1)}, s32[8,2]{0,1:T(2,128)}, u32[]{:S(2)}) copy-start(s32[8,2]{0,1:T(2,128)} %param.42) | copy-start | bytes 196
  0.7 39.1 %copy-start.4 = (f32[8,4]{0,1:T(4,128)S(1)}, f32[8,4]{0,1:T(4,128)}, u32[]{:S(2)}) copy-start(f32[8,4]{0,1:T(4,128)} %param.43) | copy-start | bytes 388
  0.7 39.1 %copy-start.6 = (f32[8,2]{0,1:T(2,128)S(1)}, f32[8,2]{0,1:T(2,128)}, u32[]{:S(2)}) copy-start(f32[8,2]{0,1:T(2,128)} %param.44) | copy-start | bytes 196
  0.7 43.8 %copy-start.5 = (bf16[1024]{0:T(1024)(128)(2,1)S(1)}, bf16[1024]{0:T(1024)(128)(2,1)}, u32[]{:S(2)}) copy-start(bf16[1024]{0:T(1024)(128)(2,1)} %param.39) | copy-start | bytes 6148
  27.5 16.9 %all-to-all-start.1 = ((bf16[16,1,128]{2,1,0:T(2,128)(2,1)}), bf16[16,1,128]{2,1,0:T(2,128)(2,1)S(1)}, u32[]{:S(2)}, u32[]{:S(2)}) async-start(bf16[16,1,128]{2,1,0:T(2,128)(2,1)} %copy.61), calls=%async_computation.1 | async-start | bytes 16384 | tf_op jit(solution)/shard_map/all_to_all | solution.py:87
  44.5 12.3 %all-to-all-start = ((bf16[16,1,128]{2,1,0:T(2,128)(2,1)}), bf16[16,1,128]{2,1,0:T(2,128)(2,1)S(1)}, u32[]{:S(2)}, u32[]{:S(2)}) async-start(bf16[16,1,128]{2,1,0:T(2,128)(2,1)} %copy.59), calls=%async_computation | async-start | bytes 16384 | tf_op jit(solution)/shard_map/all_to_all | solution.py:86
  56.8 9.8 %all-to-all-start.2 = ((bf16[16,2,128]{2,1,0:T(2,128)(2,1)}), bf16[16,2,128]{2,1,0:T(2,128)(2,1)S(1)}, u32[]{:S(2)}, u32[]{:S(2)}) async-start(bf16[16,2,128]{2,1,0:T(2,128)(2,1)} %reshape.328), calls=%async_computation.2 | async-start | bytes 16384 | tf_op jit(solution)/shard_map/all_to_all | solution.py:88
  66.6 11.3 %all-to-all-start.3 = ((bf16[16,2,128]{2,1,0:T(2,128)(2,1)}), bf16[16,2,128]{2,1,0:T(2,128)(2,1)S(1)}, u32[]{:S(2)}, u32[]{:S(2)}) async-start(bf16[16,2,128]{2,1,0:T(2,128)(2,1)} %reshape.326), calls=%async_computation.3 | async-start | bytes 16384 | tf_op jit(solution)/shard_map/all_to_all | solution.py:89
  73.7 2.0 %copy-start.1 = (f32[2,512,1024]{2,1,0:T(8,128)}, f32[2,512,1024]{2,1,0:T(8,128)S(1)}, u32[]{:S(2)}) copy-start(f32[2,512,1024]{2,1,0:T(8,128)S(1)} %multiply_add_fusion) | copy-start | bytes 12582916
  73.8 27.0 %copy-start.2 = (bf16[8,256]{1,0:T(8,128)(2,1)S(1)}, bf16[8,256]{1,0:T(8,128)(2,1)}, u32[]{:S(2)}) copy-start(bf16[8,256]{1,0:T(8,128)(2,1)} %param.29) | copy-start | bytes 12292
  167.1 10.0 %all-to-all-start.4 = ((bf16[16,2,256]{2,1,0:T(2,128)(2,1)}), bf16[16,2,256]{2,1,0:T(2,128)(2,1)S(1)}, u32[]{:S(2)}, u32[]{:S(2)}) async-start(bf16[16,2,256]{2,1,0:T(2,128)(2,1)} %constant_dynamic-update-slice_fusion), calls=%async_computation.4 | async-start | bytes 32768 | tf_op jit(solution)/shard_map/all_to_all | solution.py:156
